TPU v7x, 32 devices: a whole 2x2x4 slice. The times are simulated.
32 devices in a mesh: kv: 8 (over z, x), tp: 4 (over y, core).
Axes of the slice: x: 2, y: 2, z: 4, core: 2. Of those that a mesh axis runs over, the one named last changes fastest.
Arguments:
- tokens: bfloat16 [128, 2048], P(None, 'kv'), may hold values from -16 to 16
- norm_gain: bfloat16 [2048], P('kv'), may hold values from 0.099609375 to 1.8984375
- w_query: bfloat16 [2048, 1024], P('kv', 'tp'), may hold values from -0.125 to 0.125
- w_key: bfloat16 [2048, 1024], P('kv', 'tp'), may hold values from -0.125 to 0.125
- w_value: bfloat16 [2048, 2048], P('kv', 'tp'), may hold values from -0.125 to 0.125
- w_gate: bfloat16 [2048, 2048], P('kv', 'tp'), may hold values from -0.125 to 0.125
- w_decay: bfloat16 [2048, 1024], P('kv', 'tp'), may hold values from -0.5 to 0.5
- log_decay: float32 [128, 1024], P('kv', 'tp'), may hold values from -1.5 to 0
- state: float32 [128, 8, 128, 256], P('kv', 'tp'), may hold values from -6 to 6
- out_gain: float32 [256], replicated, may hold values from 0.1 to 1.9
- w_out: bfloat16 [2048, 2048], P('tp', 'kv'), may hold values from -0.125 to 0.125
- mixer_gain: bfloat16 [2048], P('kv'), may hold values from 0.099609375 to 1.8984375
- w_ffgate: bfloat16 [2048, 6144], P('kv', 'tp'), may hold values from -0.125 to 0.125
- w_ffup: bfloat16 [2048, 6144], P('kv', 'tp'), may hold values from -0.125 to 0.125
- w_down: bfloat16 [6144, 2048], P('tp', 'kv'), may hold values from -0.078125 to 0.078125
Outputs:
- result: bfloat16 [128, 2048], P(None, 'kv')
- new_state: float32 [128, 8, 128, 256], P('kv', 'tp')
All inputs are finite; a program needn't handle non-finite values.
Results may differ from a plain program's by a relative error of at most 0.028.
Values may be sent and summed in bfloat16 or wider, within the bound.
A program may use at most 64 MiB of HBM per device.

v0:
```python
import jax
import jax.numpy as jnp
from jax import lax
from jax.sharding import PartitionSpec as P

D = 2048
DK = 128
DV = 256


eps = 1e-06
gate_norm = 16.0


def prepare(resid, gain):
    wide = resid.astype(jnp.float32)
    scaled = (wide * gain.astype(jnp.float32)).astype(jnp.bfloat16)
    return (scaled, jnp.sum(wide * wide, axis=1))


def project(scaled, weights):
    return jnp.concatenate(
        [jnp.dot(scaled, weight, preferred_element_type=jnp.float32) for weight in weights], axis=1
    )


def activate(terms, sums, width):
    terms = terms * lax.rsqrt(sums / D + eps)[:, None]
    return (jax.nn.silu(terms[:, :width]) * terms[:, width:]).astype(jnp.bfloat16)


def body(
    tokens,
    norm_gain,
    w_query,
    w_key,
    w_value,
    w_gate,
    w_decay,
    log_decay,
    state,
    out_gain,
    w_out,
    mixer_gain,
    w_ffgate,
    w_ffup,
    w_down,
):
    seq_dev = state.shape[0]
    heads = state.shape[1]
    key_width = w_query.shape[1]
    value_width = w_value.shape[1]
    scaled, squares = prepare(tokens, norm_gain)
    attn_weights = (w_query, w_key, w_value, w_gate, w_decay)
    sums_all = lax.psum(squares, "kv")
    terms = lax.psum_scatter(
        project(scaled, attn_weights).astype(jnp.bfloat16), "kv", scatter_dimension=0, tiled=True
    ).astype(jnp.float32)
    sums = lax.dynamic_slice_in_dim(sums_all, lax.axis_index("kv") * seq_dev, seq_dev, 0)
    terms = terms * lax.rsqrt(sums / D + eps)[:, None]
    query = terms[:, :key_width].reshape(seq_dev, heads, DK) * DK ** (-0.5)
    keys = terms[:, key_width : 2 * key_width].reshape(seq_dev, heads, DK)
    values = terms[:, 2 * key_width : 2 * key_width + value_width].reshape(seq_dev, heads, DV)
    gate = terms[:, 2 * key_width + value_width : 2 * key_width + 2 * value_width]
    decay_pre = terms[:, 2 * key_width + 2 * value_width :]
    log_a = jax.nn.log_sigmoid(decay_pre) / gate_norm + log_decay
    new_state = (
        state * jnp.exp(log_a).reshape(seq_dev, heads, DK)[..., None]
        + keys[..., None] * values[:, :, None, :]
    )
    attended = jnp.einsum("bhk,bhkv->bhv", query, new_state, precision=lax.Precision.HIGHEST)
    normed = (
        attended * lax.rsqrt(jnp.mean(attended * attended, axis=2, keepdims=True) + eps) * out_gain
    )
    mixed = (normed.reshape(seq_dev, value_width) * jax.nn.silu(gate)).astype(jnp.bfloat16)
    partial_out = jnp.dot(
        lax.all_gather(mixed, "kv", axis=0, tiled=True), w_out, preferred_element_type=jnp.float32
    )
    attn_sum = lax.psum(partial_out.astype(jnp.bfloat16), "tp").astype(jnp.float32)
    middle = (tokens.astype(jnp.float32) + attn_sum).astype(jnp.bfloat16)
    scaled2, squares2 = prepare(middle, mixer_gain)
    ff_weights = (w_ffgate, w_ffup)
    width = w_ffgate.shape[1]
    terms2, sums2 = (
        lax.psum(project(scaled2, ff_weights).astype(jnp.bfloat16), "kv").astype(jnp.float32),
        lax.psum(squares2.astype(jnp.bfloat16), "kv").astype(jnp.float32),
    )
    hidden = activate(terms2, sums2, width)
    partial_down = jnp.dot(hidden, w_down, preferred_element_type=jnp.float32)
    down_total = lax.psum(partial_down.astype(jnp.bfloat16), "tp").astype(jnp.float32)
    result = (middle.astype(jnp.float32) + down_total).astype(jnp.bfloat16)
    return (result, new_state)


def solution(mesh):
    return jax.shard_map(
        body,
        mesh=mesh,
        in_specs=(
            P(None, "kv"),
            P("kv"),
            P("kv", "tp"),
            P("kv", "tp"),
            P("kv", "tp"),
            P("kv", "tp"),
            P("kv", "tp"),
            P("kv", "tp"),
            P("kv", "tp", None, None),
            P(),
            P("tp", "kv"),
            P("kv"),
            P("kv", "tp"),
            P("kv", "tp"),
            P("tp", "kv"),
        ),
        out_specs=(P(None, "kv"), P("kv", "tp", None, None)),
        check_vma=False,
    )
```

profile of v0, /device:TPU:1, one launch (start us, length us, event | category | flops | bytes accessed | tf_op | source)
XLA Modules:
  0.0 268.9 jit_solution(2558215234920750995)
XLA Ops:
  7.2 0.7 convert_element_type.59
  7.9 1.1 fusion.4
  9.1 1.1 fusion.3
  10.2 1.2 fusion.1
  11.4 1.2 fusion
  12.5 1.1 fusion.2
  13.7 0.8 copy-done.4
  14.5 0.9 fusion.8
  15.4 18.7 %psum.35 = f32[128]{0:T(128)S(1)} all-reduce(f32[128]{0:T(128)S(1)} %fusion.8), channel_id=1, replica_groups=mesh['kv'=8,'tp'=4] {'kv'}, use_global_device_ids=true, to_apply=%region_2.0 | all-reduce | flops 128 | bytes 1024 | tf_op jit(solution)/shard_map/psum | solution.py:55
  34.2 0.1 add_rsqrt_fusion.2
  34.2 43.0 %reduce-scatter.2.cloned.1.call-done = bf16[16,1792]{1,0:T(8,128)(2,1)} async-done(((bf16[128,1792]{1,0:T(8,128)(2,1)}), bf16[16,1792]{1,0:T(8,128)(2,1)}) %reduce-scatter.2.cloned.1.call-update) | async-done | bytes 57360 | tf_op jit(solution)/shard_map/reduce_scatter | solution.py:56
  77.2 0.9 convert_multiply_fusion.5
  78.2 0.7 fusion.25
  79.0 2.9 %multiply_add_fusion = f32[16,2,128,256]{3,2,1,0:T(8,128)S(1)} fusion(f32[16,2,128,256]{3,2,1,0:T(8,128)} %param.23, f32[16,2,256]{2,1,0:T(2,128)S(1)} %mul.124, f32[16,2,128]{2,1,0:T(2,128)S(1)} %mul.122, f32[16,2,128]{2,1,0:T(2,128)S(1)} %mul.119), kind=kLoop, calls=%fused_computation | loop fusion | flops 3145728 | bytes 8454144 | tf_op jit(solution)/shard_map/add | solution.py:68
  81.9 1.9 copy-done.1
  83.9 2.1 fusion.28
  86.0 0.1 fusion.15
  86.1 0.1 fusion.16
  86.2 24.4 %all_gather.3 = bf16[128,512]{1,0:T(8,128)(2,1)S(1)} all-gather(bf16[16,512]{1,0:T(8,128)(2,1)S(1)} %multiply_convert_fusion), channel_id=1, replica_groups=mesh['kv'=8,'tp'=4] {'kv'}, dimensions={0}, use_global_device_ids=true | all-gather | bytes 147456 | tf_op jit(solution)/shard_map/all_gather | solution.py:77
  110.7 0.8 convolution_convert_fusion.5
  111.5 0.0 all-reduce.6.cloned.1.call-start
  111.6 37.2 %all-reduce.4.cloned.1.call-done = bf16[128,256]{1,0:T(8,128)(2,1)} async-done(((bf16[128,256]{1,0:T(8,128)(2,1)}), bf16[128,256]{1,0:T(8,128)(2,1)}) %all-reduce.4.cloned.1.call-update) | async-done | bytes 65552 | tf_op jit(solution)/shard_map/psum | solution.py:79
  148.8 0.9 fusion.11
  149.8 0.3 convolution_convert_fusion
  150.0 0.3 convolution_convert_fusion.1
  150.3 1.0 pad_maximum_fusion
  151.4 18.2 %psum.38 = bf16[128]{0:T(256)(128)(2,1)S(1)} all-reduce(bf16[128]{0:T(256)(128)(2,1)S(1)} %get-tuple-element.2), channel_id=1, replica_groups=mesh['kv'=8,'tp'=4] {'kv'}, use_global_device_ids=true, to_apply=%region_7.8 | all-reduce | flops 128 | bytes 512 | tf_op jit(solution)/shard_map/psum | solution.py:86
  169.6 58.1 %all-reduce.6.cloned.1.call-done = bf16[128,3072]{1,0:T(8,128)(2,1)} async-done(((bf16[128,3072]{1,0:T(8,128)(2,1)}), bf16[128,3072]{1,0:T(8,128)(2,1)}) %all-reduce.6.cloned.1.call-update) | async-done | bytes 786448 | tf_op jit(solution)/shard_map/psum | solution.py:85
  227.7 1.3 convert_multiply_fusion
  229.0 1.0 convolution_convert_fusion.4
  230.1 30.8 %all-reduce.8.cloned.1.call-done = bf16[128,256]{1,0:T(8,128)(2,1)} async-done(((bf16[128,256]{1,0:T(8,128)(2,1)}), bf16[128,256]{1,0:T(8,128)(2,1)}) %all-reduce.8.cloned.1.call-update) | async-done | bytes 65552 | tf_op jit(solution)/shard_map/psum | solution.py:90
  260.9 1.5 fusion.12
  (33 shorter events, 0.4 us)
Async XLA Ops:
  7.2 142.6 %copy-start = (bf16[256,1536]{1,0:T(8,128)(2,1)S(1)}, bf16[256,1536]{1,0:T(8,128)(2,1)}, u32[]{:S(2)}) copy-start(bf16[256,1536]{1,0:T(8,128)(2,1)} %param.28) | copy-start | bytes 2359300
  7.2 70.1 %reduce-scatter.2.cloned.1.call-start = ((), (), s32[]{:S(2)}) async-start(), calls=%async_computation.1 | async-start | bytes 516096 | tf_op jit(solution)/shard_map/reduce_scatter | solution.py:56
  13.6 0.8 copy-start.4
  14.4 134.4 %all-reduce.4.cloned.1.call-start = ((), (), s32[]{:S(2)}) async-start(), calls=%async_computation.2 | async-start | bytes 131072 | tf_op jit(solution)/shard_map/psum | solution.py:79
  81.8 2.0 copy-start.1
  81.9 4.2 %copy-start.6 = (f32[256]{0:T(256)S(1)}, f32[256]{0:T(256)}, u32[]{:S(2)}) copy-start(f32[256]{0:T(256)} %param.24) | copy-start | bytes 3076
  81.9 28.8 %copy-start.5 = (bf16[512,256]{1,0:T(8,128)(2,1)S(1)}, bf16[512,256]{1,0:T(8,128)(2,1)}, u32[]{:S(2)}) copy-start(bf16[512,256]{1,0:T(8,128)(2,1)} %param.25) | copy-start | bytes 786436
  81.9 29.7 %copy-start.8 = (bf16[256]{0:T(256)(128)(2,1)S(1)}, bf16[256]{0:T(256)(128)(2,1)}, u32[]{:S(2)}) copy-start(bf16[256]{0:T(256)(128)(2,1)} %param.26) | copy-start | bytes 1540
  81.9 66.9 %copy-start.2 = (bf16[128,256]{1,0:T(8,128)(2,1)S(1)}, bf16[128,256]{1,0:T(8,128)(2,1)}, u32[]{:S(2)}) copy-start(bf16[128,256]{1,0:T(8,128)(2,1)} %param.15) | copy-start | bytes 196612
  81.9 68.1 %copy-start.3 = (bf16[256,1536]{1,0:T(8,128)(2,1)S(1)}, bf16[256,1536]{1,0:T(8,128)(2,1)}, u32[]{:S(2)}) copy-start(bf16[256,1536]{1,0:T(8,128)(2,1)} %param.27) | copy-start | bytes 2359300
  86.0 143.1 %copy-start.7 = (bf16[1536,256]{1,0:T(8,128)(2,1)S(1)}, bf16[1536,256]{1,0:T(8,128)(2,1)}, u32[]{:S(2)}) copy-start(bf16[1536,256]{1,0:T(8,128)(2,1)} %param.29) | copy-start | bytes 2359300
  111.5 116.2 %all-reduce.6.cloned.1.call-start = ((), (), s32[]{:S(2)}) async-start(), calls=%async_computation.3 | async-start | bytes 1572864 | tf_op jit(solution)/shard_map/psum | solution.py:85
  151.3 109.5 %all-reduce.8.cloned.1.call-start = ((), (), s32[]{:S(2)}) async-start(), calls=%async_computation.4 | async-start | bytes 131072 | tf_op jit(solution)/shard_map/psum | solution.py:90
Sparse Core Ops, SparseCore 0:
  14.6 62.6 reduce-scatter.1
  111.6 37.1 all-reduce.3
  152.2 75.4 all-reduce.5
  230.4 30.3 all-reduce.7
where the time goes:
time: 272 us; the launch traced here: 269 us
  waiting for transfers between devices  169 us (62%)
  blocking collectives  61.4 us (23%)
  between operations  14 us (5%)
  other arithmetic  11.2 us (4%)
  matrix products  10.1 us (4%)
  local copies, waits for them, and re-layouts  2.83 us (1%)
    psum x1, waiting for transfers between devices, body(): lax.psum(project(scaled2, ff_weights).astype(jnp.bfloat16), 'kv')  58.1 us
    reduce_scatter x1, waiting for transfers between devices, body(): lax.psum_scatter(project(scaled, attn_weights).astype(jnp.bfloat16), 'kv'...  43 us
    psum x1, waiting for transfers between devices, body(): lax.psum(partial_out.astype(jnp.bfloat16), 'tp').astype(jnp.float32)  37.2 us
    psum x1, waiting for transfers between devices, body(): lax.psum(partial_down.astype(jnp.bfloat16), 'tp').astype(jnp.float32)  30.8 us
    all_gather x1, blocking collectives, body(): lax.all_gather(mixed, 'kv', axis=0, tiled=True)  24.4 us
    psum x1, blocking collectives, body(): sums_all = lax.psum(squares, 'kv')  18.7 us
    psum x1, blocking collectives, body(): lax.psum(squares2.astype(jnp.bfloat16), 'kv').astype(jnp.float32)  18.2 us
    dot_general x7, matrix products, project(): jnp.dot(scaled, weight, preferred_element_type=jnp.float32)  6.19 us
  transfers between devices with their start and end apart: 4, of which 4 were waited for; matrix products, arithmetic and copies ran while one was open for 0% of the time, Pallas kernels for 0%

commit v1 on v0

v1 whole, which is shorter than its diff:
```python
import functools

import jax
import jax.numpy as jnp
from jax import lax
from jax.experimental import pallas as pl
from jax.experimental.pallas import tpu as pltpu
from jax.sharding import PartitionSpec as P

eps = 1e-06
gate_norm = 16.0
LANES = 128
F32 = jnp.float32
BF16 = jnp.bfloat16


def remote(src, dst, send_sem, recv_sem, device):
    return pltpu.make_async_remote_copy(
        src_ref=src,
        dst_ref=dst,
        send_sem=send_sem,
        recv_sem=recv_sem,
        device_id=device,
        device_id_type=pl.DeviceIdType.MESH,
    )


def split_axis(n_kv):
    n_in = 1
    while n_in * n_in * 4 <= n_kv:
        n_in *= 2
    return n_kv // n_in, n_in


def ff_chunks(width):
    tiles = max(width // LANES, 1)
    return max(n for n in (1, 2, 3, 4) if tiles % n == 0)


def kernel(
    n_kv,
    n_tp,
    d_model,
    tokens_ref,
    norm_gain_ref,
    wq_hbm,
    wk_hbm,
    wv_hbm,
    wg_hbm,
    wd_hbm,
    log_decay_ref,
    state_hbm,
    out_gain_ref,
    wo_hbm,
    mixer_gain_ref,
    wfg_hbm,
    wfu_hbm,
    wdn_hbm,
    result_ref,
    ns_ref,
    wq,
    wk,
    wv,
    wg,
    wd,
    wo,
    wfg,
    wfu,
    wdn,
    px,
    rx,
    pz,
    rz,
    att,
    mg,
    to,
    fx,
    frx,
    fz,
    frz,
    hg,
    td,
    middle_ref,
    load_sem,
    ax_s,
    ax_r,
    az_s,
    az_r,
    mz_s,
    mz_r,
    mx_s,
    mx_r,
    to_s,
    to_r,
    fx_s,
    fx_r,
    fz_s,
    fz_r,
    hz_s,
    hz_r,
    hx_s,
    hx_r,
    td_s,
    td_r,
):
    n_out, n_in = split_axis(n_kv)
    kv = lax.axis_index("kv")
    tp = lax.axis_index("tp")
    zi = kv // n_in
    xi = lax.rem(kv, n_in)
    rows = px.shape[2]
    batch = tokens_ref.shape[0]

    def x_peer(d):
        return lax.rem(xi + d, n_in)

    def z_peer(d):
        return lax.rem(zi + d, n_out)

    def z_back(d):
        return lax.rem(zi + n_out - d, n_out)

    def x_back(d):
        return lax.rem(xi + n_in - d, n_in)

    def x_dev(d):
        return (zi * n_in + x_peer(d), tp)

    def z_dev(d):
        return (z_peer(d) * n_in + xi, tp)

    def t_dev(d):
        return (kv, lax.rem(tp + d, n_tp))

    barrier = pltpu.get_barrier_semaphore()
    peers = (
        [x_dev(d) for d in range(1, n_in)]
        + [z_dev(d) for d in range(1, n_out)]
        + [t_dev(d) for d in range(1, n_tp)]
    )
    for dev in peers:
        pl.semaphore_signal(barrier, inc=1, device_id=dev, device_id_type=pl.DeviceIdType.MESH)

    loads = [
        pltpu.make_async_copy(src, dst, load_sem.at[i])
        for i, (src, dst) in enumerate(
            (
                (wq_hbm, wq),
                (wk_hbm, wk),
                (wd_hbm, wd),
                (wv_hbm, wv),
                (wg_hbm, wg),
                (state_hbm, ns_ref),
                (wo_hbm, wo),
                (wfg_hbm, wfg),
                (wfu_hbm, wfu),
                (wdn_hbm, wdn),
            )
        )
    ]
    for load in loads:
        load.start()
    load_q, load_k, load_d, load_v, load_g, load_state, load_o, load_fg, load_fu, load_dn = loads

    pending = []

    def launch(copy):
        copy.start()
        pending.append(copy)

    def scatter_rows(dst, value, lo):
        width = value.shape[1]
        value = value.astype(BF16)
        for z in range(n_out):
            for x in range(n_in):
                at = (z * n_in + x) * rows
                dst[x, z, :, lo : lo + width] = value[at : at + rows]

    def send_x(src, dst, s, r, c, lo, hi):
        cols = slice(lo, hi)
        return [
            remote(
                src.at[x_peer(d), :, :, cols],
                dst.at[d - 1, :, :, cols],
                s.at[c, d - 1],
                r.at[c, d - 1],
                x_dev(d),
            )
            for d in range(1, n_in)
        ]

    def send_z(src, dst, s, r, c, lo, hi):
        cols = slice(lo, hi)
        return [
            remote(
                src.at[z_peer(d), :, cols],
                dst.at[d - 1, :, cols],
                s.at[c, d - 1],
                r.at[c, d - 1],
                z_dev(d),
            )
            for d in range(1, n_out)
        ]

    def reduce_x(src, got, dst, copies, lo, hi):
        for copy in copies:
            copy.wait_recv()
        total = src[xi, :, :, lo:hi].astype(F32)
        for d in range(1, n_in):
            total = total + got[d - 1, :, :, lo:hi].astype(F32)
        dst[:, :, lo:hi] = total.astype(BF16)

    def reduce_z(src, got, copies, lo, hi):
        for copy in copies:
            copy.wait_recv()
        total = src[zi, :, lo:hi].astype(F32)
        for d in range(1, n_out):
            total = total + got[d - 1, :, lo:hi].astype(F32)
        return total

    wide = tokens_ref[...].astype(F32)
    scaled = (wide * norm_gain_ref[...].astype(F32).reshape(1, -1)).astype(BF16)
    squares = jnp.broadcast_to(jnp.sum(wide * wide, axis=1, keepdims=True), (batch, LANES))

    kw = wq.shape[1]
    vw = wv.shape[1]
    q_at = LANES
    k_at = q_at + kw
    d_at = k_at + kw
    v_at = d_at + kw
    g_at = v_at + vw
    end = g_at + vw
    bounds = ((0, d_at), (d_at, g_at), (g_at, end))
    parts = (
        ((wq, load_q, q_at), (wk, load_k, k_at)),
        ((wd, load_d, d_at), (wv, load_v, v_at)),
        ((wg, load_g, g_at),),
    )
    x_copies = []
    for c, ((lo, hi), part) in enumerate(zip(bounds, parts)):
        if c == 0:
            scatter_rows(px, squares, 0)
        for weight, load, at in part:
            load.wait()
            scatter_rows(px, jnp.dot(scaled, weight[...], preferred_element_type=F32), at)
        if c == 0:
            pl.semaphore_wait(barrier, len(peers))
        copies = send_x(px, rx, ax_s, ax_r, c, lo, hi)
        for copy in copies:
            launch(copy)
        x_copies.append(copies)
    z_copies = []
    for c, (lo, hi) in enumerate(bounds):
        reduce_x(px, rx, pz, x_copies[c], lo, hi)
        copies = send_z(pz, rz, az_s, az_r, c, lo, hi)
        for copy in copies:
            launch(copy)
        z_copies.append(copies)

    first = reduce_z(pz, rz, z_copies[0], *bounds[0])
    inv = lax.rsqrt(first[:, :1] / d_model + eps)
    second = reduce_z(pz, rz, z_copies[1], *bounds[1])

    heads, dk, dv = ns_ref.shape[1:]
    query = first[:, q_at : q_at + kw] * inv * dk ** (-0.5)
    keys = first[:, k_at : k_at + kw] * inv
    pre = second[:, :kw] * inv
    values = second[:, kw:] * inv
    log_sig = jnp.minimum(pre, 0.0) - jnp.log1p(jnp.exp(-jnp.abs(pre)))
    decay = jnp.exp(log_sig / gate_norm + log_decay_ref[...])
    load_state.wait()
    for h in range(heads):
        ks = slice(h * dk, (h + 1) * dk)
        q_t = query[:, ks].T
        k_t = keys[:, ks].T
        a_t = decay[:, ks].T
        for b in range(rows):
            col = slice(b, b + 1)
            v_row = values[b : b + 1, h * dv : (h + 1) * dv]
            new = ns_ref[b, h] * a_t[:, col] + k_t[:, col] * v_row
            ns_ref[b, h] = new
            att[h, b : b + 1, :] = jnp.sum(new * q_t[:, col], axis=0, keepdims=True)

    gate = reduce_z(pz, rz, z_copies[2], *bounds[2]) * inv
    for h in range(heads):
        got = att[h]
        normed = (
            got
            * lax.rsqrt(jnp.mean(got * got, axis=1, keepdims=True) + eps)
            * out_gain_ref[...]
        )
        cols = slice(h * dv, (h + 1) * dv)
        mg[zi, xi, :, cols] = (normed * jax.nn.silu(gate[:, cols])).astype(BF16)

    def gather_z(buf, s, r):
        for d in range(1, n_out):
            launch(remote(buf.at[zi, xi], buf.at[zi, xi], s.at[d - 1], r.at[d - 1], z_dev(d)))

    def forward_x(buf, zs, zr, s, r):
        for dz in range(n_out):
            slot = buf.at[z_back(dz), xi]
            if dz:
                remote(slot, slot, zs.at[dz - 1], zr.at[dz - 1], z_dev(dz)).wait_recv()
            for d in range(1, n_in):
                launch(remote(slot, slot, s.at[dz, d - 1], r.at[dz, d - 1], x_dev(d)))

    def arrive_x(buf, s, r):
        for dz in range(n_out):
            for d in range(1, n_in):
                slot = buf.at[z_back(dz), x_back(d)]
                remote(slot, slot, s.at[dz, d - 1], r.at[dz, d - 1], x_dev(d)).wait_recv()

    gather_z(mg, mz_s, mz_r)
    forward_x(mg, mz_s, mz_r, mx_s, mx_r)
    load_o.wait()
    arrive_x(mg, mx_s, mx_r)

    def sum_groups(buf, s, r):
        for d in range(1, n_tp):
            launch(remote(buf.at[tp], buf.at[tp], s.at[d - 1], r.at[d - 1], t_dev(d)))
        for d in range(1, n_tp):
            slot = buf.at[lax.rem(tp + n_tp - d, n_tp)]
            remote(slot, slot, s.at[d - 1], r.at[d - 1], t_dev(d)).wait_recv()
        total = buf[0].astype(F32)
        for g in range(1, n_tp):
            total = total + buf[g].astype(F32)
        return total

    mixed = mg[...].reshape(batch, vw)
    to[tp] = jnp.dot(mixed, wo[...], preferred_element_type=F32).astype(BF16)
    middle = (tokens_ref[...].astype(F32) + sum_groups(to, to_s, to_r)).astype(BF16)
    middle_ref[...] = middle

    wide2 = middle.astype(F32)
    scaled2 = (wide2 * mixer_gain_ref[...].astype(F32).reshape(1, -1)).astype(BF16)
    squares2 = jnp.broadcast_to(jnp.sum(wide2 * wide2, axis=1, keepdims=True), (batch, LANES))
    ff = wfg.shape[1]
    n_c = ff_chunks(ff)
    fc = ff // n_c
    fbounds = [
        (0 if c == 0 else LANES + 2 * fc * c, LANES + 2 * fc * (c + 1)) for c in range(n_c)
    ]
    load_fg.wait()
    load_fu.wait()
    fx_copies = []
    for c, (lo, hi) in enumerate(fbounds):
        if c == 0:
            scatter_rows(fx, squares2, 0)
        cols = slice(c * fc, (c + 1) * fc)
        at = LANES + 2 * fc * c
        scatter_rows(fx, jnp.dot(scaled2, wfg[:, cols], preferred_element_type=F32), at)
        scatter_rows(fx, jnp.dot(scaled2, wfu[:, cols], preferred_element_type=F32), at + fc)
        copies = send_x(fx, frx, fx_s, fx_r, c, lo, hi)
        for copy in copies:
            launch(copy)
        fx_copies.append(copies)

    fz_copies = [None] * n_c
    inv2 = [None]

    def to_z(c):
        lo, hi = fbounds[c]
        reduce_x(fx, frx, fz, fx_copies[c], lo, hi)
        fz_copies[c] = send_z(fz, frz, fz_s, fz_r, c, lo, hi)
        for copy in fz_copies[c]:
            launch(copy)

    def activate(c):
        terms = reduce_z(fz, frz, fz_copies[c], *fbounds[c])
        if c == 0:
            inv2[0] = lax.rsqrt(terms[:, :1] / d_model + eps)
            terms = terms[:, LANES:]
        terms = terms * inv2[0]
        hg[c, zi, xi] = (jax.nn.silu(terms[:, :fc]) * terms[:, fc:]).astype(BF16)
        gather_z(hg.at[c], hz_s.at[c], hz_r.at[c])

    def hand_on(c):
        forward_x(hg.at[c], hz_s.at[c], hz_r.at[c], hx_s.at[c], hx_r.at[c])

    for t in range(n_c + 3):
        if t < n_c:
            to_z(t)
        if 0 <= t - 2 < n_c:
            activate(t - 2)
        if 0 <= t - 3 < n_c:
            hand_on(t - 3)

    load_dn.wait()
    down = None
    for c in range(n_c):
        arrive_x(hg.at[c], hx_s.at[c], hx_r.at[c])
        term = jnp.dot(
            hg[c].reshape(batch, fc),
            wdn[c * fc : (c + 1) * fc, :],
            preferred_element_type=F32,
        )
        down = term if down is None else down + term
    td[tp] = down.astype(BF16)
    total = sum_groups(td, td_s, td_r)
    result_ref[...] = (middle_ref[...].astype(F32) + total).astype(BF16)

    for copy in pending:
        copy.wait_send()


def body(n_kv, n_tp, *args):
    (
        tokens,
        norm_gain,
        w_query,
        w_key,
        w_value,
        w_gate,
        w_decay,
        log_decay,
        state,
        out_gain,
        w_out,
        mixer_gain,
        w_ffgate,
        w_ffup,
        w_down,
    ) = args
    n_out, n_in = split_axis(n_kv)
    batch, feats = tokens.shape
    rows, heads, dk, dv = state.shape
    kw = w_query.shape[1]
    vw = w_value.shape[1]
    ff = w_ffgate.shape[1]
    n_c = ff_chunks(ff)
    fc = ff // n_c
    width = LANES + 3 * kw + 2 * vw
    fwidth = LANES + 2 * ff
    m_in, m_out, m_tp = max(n_in - 1, 1), max(n_out - 1, 1), max(n_tp - 1, 1)
    dma = pltpu.SemaphoreType.DMA
    vmem = pltpu.VMEM
    whole = pl.BlockSpec(memory_space=pltpu.VMEM)
    far = pl.BlockSpec(memory_space=pl.ANY)
    sems = [
        (10,),
        (3, m_in),
        (3, m_in),
        (3, m_out),
        (3, m_out),
        (m_out,),
        (m_out,),
        (n_out, m_in),
        (n_out, m_in),
        (m_tp,),
        (m_tp,),
        (n_c, m_in),
        (n_c, m_in),
        (n_c, m_out),
        (n_c, m_out),
        (n_c, m_out),
        (n_c, m_out),
        (n_c, n_out, m_in),
        (n_c, n_out, m_in),
        (m_tp,),
        (m_tp,),
    ]
    result, new_state = pl.pallas_call(
        functools.partial(kernel, n_kv, n_tp, feats * n_kv),
        out_shape=(
            vmem((batch, feats), BF16),
            vmem(state.shape, F32),
        ),
        in_specs=[
            whole,
            whole,
            far,
            far,
            far,
            far,
            far,
            whole,
            far,
            whole,
            far,
            whole,
            far,
            far,
            far,
        ],
        out_specs=(whole, whole),
        scratch_shapes=[
            vmem(w_query.shape, BF16),
            vmem(w_key.shape, BF16),
            vmem(w_value.shape, BF16),
            vmem(w_gate.shape, BF16),
            vmem(w_decay.shape, BF16),
            vmem(w_out.shape, BF16),
            vmem(w_ffgate.shape, BF16),
            vmem(w_ffup.shape, BF16),
            vmem(w_down.shape, BF16),
            vmem((n_in, n_out, rows, width), BF16),
            vmem((m_in, n_out, rows, width), BF16),
            vmem((n_out, rows, width), BF16),
            vmem((m_out, rows, width), BF16),
            vmem((heads, rows, dv), F32),
            vmem((n_out, n_in, rows, vw), BF16),
            vmem((n_tp, batch, feats), BF16),
            vmem((n_in, n_out, rows, fwidth), BF16),
            vmem((m_in, n_out, rows, fwidth), BF16),
            vmem((n_out, rows, fwidth), BF16),
            vmem((m_out, rows, fwidth), BF16),
            vmem((n_c, n_out, n_in, rows, fc), BF16),
            vmem((n_tp, batch, feats), BF16),
            vmem((batch, feats), BF16),
        ]
        + [dma(shape) for shape in sems],
        compiler_params=pltpu.CompilerParams(
            collective_id=0, has_side_effects=True, vmem_limit_bytes=56 * 2**20
        ),
    )(
        tokens,
        norm_gain,
        w_query,
        w_key,
        w_value,
        w_gate,
        w_decay,
        log_decay,
        state,
        out_gain.reshape(1, dv),
        w_out,
        mixer_gain,
        w_ffgate,
        w_ffup,
        w_down,
    )
    return (result, new_state)


def solution(mesh):
    return jax.shard_map(
        functools.partial(body, mesh.shape["kv"], mesh.shape["tp"]),
        mesh=mesh,
        in_specs=(
            P(None, "kv"),
            P("kv"),
            P("kv", "tp"),
            P("kv", "tp"),
            P("kv", "tp"),
            P("kv", "tp"),
            P("kv", "tp"),
            P("kv", "tp"),
            P("kv", "tp", None, None),
            P(),
            P("tp", "kv"),
            P("kv"),
            P("kv", "tp"),
            P("kv", "tp"),
            P("tp", "kv"),
        ),
        out_specs=(P(None, "kv"), P("kv", "tp", None, None)),
        check_vma=False,
    )
```

time: 272 us -> 62.4 us (0.23); the launches traced: 269 us -> 62.3 us
  waiting for transfers between devices: 169 us -> 0 us
  blocking collectives: 61.4 us -> 0 us
  Pallas kernels: 0 us -> 59 us
  between operations: 14 us -> 0.64 us
  other arithmetic: 11.2 us -> 0 us
  matrix products: 10.1 us -> 0 us
    psum x3 -> x0, waiting for transfers between devices: 126 us -> none  [the longest x1 58.1 us: body(): lax.psum(project(scaled2, ff_weights).astype(jnp.bfloat16), 'kv')]
    pallas_call x0 -> x1, Pallas kernels: none -> 59 us  [body(): pl.pallas_call(functools.partial(kernel, n_kv, n_tp, feats * n_kv), out_s...]
    reduce_scatter x1 -> x0, waiting for transfers between devices: 43 us -> none  [body(): lax.psum_scatter(project(scaled, attn_weights).astype(jnp.bfloat16), 'kv'...]
    psum x2 -> x0, blocking collectives: 36.9 us -> none  [the longest x1 18.7 us: body(): sums_all = lax.psum(squares, 'kv')]
    all_gather x1 -> x0, blocking collectives: 24.4 us -> none  [body(): lax.all_gather(mixed, 'kv', axis=0, tiled=True)]
    dot_general x10 -> x0, matrix products: 10.1 us -> none  [the longest x7 6.19 us: project(): jnp.dot(scaled, weight, preferred_element_type=jnp.float32)]
    add x1 -> x0, other arithmetic: 2.86 us -> none  [body(): state * jnp.exp(log_a).reshape(seq_dev, heads, DK)[..., None]]
  transfers between devices with their start and end apart: 4 -> 0, of which waited for: 4 -> 0; matrix products, arithmetic and copies ran while one was open for 0% -> 0% of each run, Pallas kernels for 0% -> 0%
where the time goes in v1:
time: 62.4 us; the launch traced here: 62.3 us
  Pallas kernels  59 us (95%)
  local copies, waits for them, and re-layouts  2.64 us (4%)
  between operations  0.64 us (1%)
    pallas_call x1, Pallas kernels, body(): pl.pallas_call(functools.partial(kernel, n_kv, n_tp, feats * n_kv), out_s...  59 us
    unnamed x2, local copies, waits for them, and re-layouts  2.64 us

profile of v1, /device:TPU:1, one launch (start us, length us, event | category | flops | bytes accessed | tf_op | source)
XLA Modules:
  0.0 62.3 jit_solution(12569481192263360225)
XLA Ops:
  0.6 59.0 %shard_map.158 = (bf16[128,256]{1,0:T(8,128)(2,1)S(1)}, f32[16,2,128,256]{3,2,1,0:T(8,128)S(1)}) custom-call(bf16[128,256]{1,0:T(8,128)(2,1)} %tokens_ref.1, bf16[256]{0:T(256)(128)(2,1)} %norm_gain_ref.1, bf16[256,256]{1,0:T(8,128)(2,1)} %wq_hbm.1, bf16[256,256]{1,0:T(8,128)(2,1)} %wk_hbm.1, bf16[256,512]{1,0:T(8,128)(2,1)} %wv_hbm.1, ...), custom_call_target="tpu_custom_call" | custom-call | tf_op jit(solution)/shard_map/pallas_call | solution.py:462
  59.6 0.6 %copy.19 = bf16[128,256]{1,0:T(8,128)(2,1)} copy(bf16[128,256]{1,0:T(8,128)(2,1)S(1)} %get-tuple-element.2) | data formatting | bytes 131072
  60.2 2.0 %copy.20 = f32[16,2,128,256]{3,2,1,0:T(8,128)} copy(f32[16,2,128,256]{3,2,1,0:T(8,128)S(1)} %get-tuple-element.3) | data formatting | bytes 8388608

commit v2 on v1

--- a/solution.py
+++ b/solution.py
@@ -10,6 +10,9 @@
 eps = 1e-06
 gate_norm = 16.0
 LANES = 128
+CHUNKS = 6
+LAG_Z = 6
+LAG_X = 8
 F32 = jnp.float32
 BF16 = jnp.bfloat16
 
@@ -33,8 +36,15 @@
 
 
 def ff_chunks(width):
-    tiles = max(width // LANES, 1)
-    return max(n for n in (1, 2, 3, 4) if tiles % n == 0)
+    if width % LANES:
+        return [(0, width)]
+    left, at, ranges = width // LANES, 0, []
+    while left:
+        take = min(left, -(-(width // LANES) // CHUNKS))
+        ranges.append((at, at + take * LANES))
+        at += take * LANES
+        left -= take
+    return ranges
 
 
 def kernel(
@@ -158,7 +168,7 @@
             )
         )
     ]
-    for load in loads:
+    for load in loads[:5]:
         load.start()
     load_q, load_k, load_d, load_v, load_g, load_state, load_o, load_fg, load_fu, load_dn = loads
 
@@ -249,6 +259,8 @@
         for copy in copies:
             launch(copy)
         x_copies.append(copies)
+    for load in loads[5:]:
+        load.start()
     z_copies = []
     for c, (lo, hi) in enumerate(bounds):
         reduce_x(px, rx, pz, x_copies[c], lo, hi)
@@ -292,28 +304,29 @@
         cols = slice(h * dv, (h + 1) * dv)
         mg[zi, xi, :, cols] = (normed * jax.nn.silu(gate[:, cols])).astype(BF16)
 
-    def gather_z(buf, s, r):
+    def gather_z(buf, cols, s, r):
         for d in range(1, n_out):
-            launch(remote(buf.at[zi, xi], buf.at[zi, xi], s.at[d - 1], r.at[d - 1], z_dev(d)))
-
-    def forward_x(buf, zs, zr, s, r):
+            own = buf.at[zi, xi, :, cols]
+            launch(remote(own, own, s.at[d - 1], r.at[d - 1], z_dev(d)))
+
+    def forward_x(buf, cols, zs, zr, s, r):
         for dz in range(n_out):
-            slot = buf.at[z_back(dz), xi]
+            slot = buf.at[z_back(dz), xi, :, cols]
             if dz:
                 remote(slot, slot, zs.at[dz - 1], zr.at[dz - 1], z_dev(dz)).wait_recv()
             for d in range(1, n_in):
                 launch(remote(slot, slot, s.at[dz, d - 1], r.at[dz, d - 1], x_dev(d)))
 
-    def arrive_x(buf, s, r):
+    def arrive_x(buf, cols, s, r):
         for dz in range(n_out):
             for d in range(1, n_in):
-                slot = buf.at[z_back(dz), x_back(d)]
+                slot = buf.at[z_back(dz), x_back(d), :, cols]
                 remote(slot, slot, s.at[dz, d - 1], r.at[dz, d - 1], x_dev(d)).wait_recv()
 
-    gather_z(mg, mz_s, mz_r)
-    forward_x(mg, mz_s, mz_r, mx_s, mx_r)
+    gather_z(mg, slice(0, vw), mz_s, mz_r)
+    forward_x(mg, slice(0, vw), mz_s, mz_r, mx_s, mx_r)
     load_o.wait()
-    arrive_x(mg, mx_s, mx_r)
+    arrive_x(mg, slice(0, vw), mx_s, mx_r)
 
     def sum_groups(buf, s, r):
         for d in range(1, n_tp):
@@ -335,19 +348,18 @@
     scaled2 = (wide2 * mixer_gain_ref[...].astype(F32).reshape(1, -1)).astype(BF16)
     squares2 = jnp.broadcast_to(jnp.sum(wide2 * wide2, axis=1, keepdims=True), (batch, LANES))
     ff = wfg.shape[1]
-    n_c = ff_chunks(ff)
-    fc = ff // n_c
-    fbounds = [
-        (0 if c == 0 else LANES + 2 * fc * c, LANES + 2 * fc * (c + 1)) for c in range(n_c)
-    ]
+    chunks = ff_chunks(ff)
+    n_c = len(chunks)
+    fbounds = [(LANES + 2 * lo if lo else 0, LANES + 2 * hi) for lo, hi in chunks]
     load_fg.wait()
     load_fu.wait()
     fx_copies = []
     for c, (lo, hi) in enumerate(fbounds):
         if c == 0:
             scatter_rows(fx, squares2, 0)
-        cols = slice(c * fc, (c + 1) * fc)
-        at = LANES + 2 * fc * c
+        cols = slice(*chunks[c])
+        fc = chunks[c][1] - chunks[c][0]
+        at = hi - 2 * fc
         scatter_rows(fx, jnp.dot(scaled2, wfg[:, cols], preferred_element_type=F32), at)
         scatter_rows(fx, jnp.dot(scaled2, wfu[:, cols], preferred_element_type=F32), at + fc)
         copies = send_x(fx, frx, fx_s, fx_r, c, lo, hi)
@@ -371,27 +383,29 @@
             inv2[0] = lax.rsqrt(terms[:, :1] / d_model + eps)
             terms = terms[:, LANES:]
         terms = terms * inv2[0]
-        hg[c, zi, xi] = (jax.nn.silu(terms[:, :fc]) * terms[:, fc:]).astype(BF16)
-        gather_z(hg.at[c], hz_s.at[c], hz_r.at[c])
+        fc = terms.shape[1] // 2
+        cols = slice(*chunks[c])
+        hg[zi, xi, :, cols] = (jax.nn.silu(terms[:, :fc]) * terms[:, fc:]).astype(BF16)
+        gather_z(hg, cols, hz_s.at[c], hz_r.at[c])
 
     def hand_on(c):
-        forward_x(hg.at[c], hz_s.at[c], hz_r.at[c], hx_s.at[c], hx_r.at[c])
-
-    for t in range(n_c + 3):
+        forward_x(hg, slice(*chunks[c]), hz_s.at[c], hz_r.at[c], hx_s.at[c], hx_r.at[c])
+
+    for t in range(n_c + LAG_X):
         if t < n_c:
             to_z(t)
-        if 0 <= t - 2 < n_c:
-            activate(t - 2)
-        if 0 <= t - 3 < n_c:
-            hand_on(t - 3)
+        if 0 <= t - LAG_Z < n_c:
+            activate(t - LAG_Z)
+        if 0 <= t - LAG_X < n_c:
+            hand_on(t - LAG_X)
 
     load_dn.wait()
     down = None
-    for c in range(n_c):
-        arrive_x(hg.at[c], hx_s.at[c], hx_r.at[c])
+    for c, (lo, hi) in enumerate(chunks):
+        arrive_x(hg, slice(*chunks[c]), hx_s.at[c], hx_r.at[c])
         term = jnp.dot(
-            hg[c].reshape(batch, fc),
-            wdn[c * fc : (c + 1) * fc, :],
+            hg[:, :, :, lo:hi].reshape(batch, hi - lo),
+            wdn[lo:hi, :],
             preferred_element_type=F32,
         )
         down = term if down is None else down + term
@@ -427,8 +441,7 @@
     kw = w_query.shape[1]
     vw = w_value.shape[1]
     ff = w_ffgate.shape[1]
-    n_c = ff_chunks(ff)
-    fc = ff // n_c
+    n_c = len(ff_chunks(ff))
     width = LANES + 3 * kw + 2 * vw
     fwidth = LANES + 2 * ff
     m_in, m_out, m_tp = max(n_in - 1, 1), max(n_out - 1, 1), max(n_tp - 1, 1)
@@ -504,7 +517,7 @@
             vmem((m_in, n_out, rows, fwidth), BF16),
             vmem((n_out, rows, fwidth), BF16),
             vmem((m_out, rows, fwidth), BF16),
-            vmem((n_c, n_out, n_in, rows, fc), BF16),
+            vmem((n_out, n_in, rows, ff), BF16),
             vmem((n_tp, batch, feats), BF16),
             vmem((batch, feats), BF16),
         ]

time: 62.4 us -> 61.8 us (level)
  Pallas kernels: 59 us -> 58.3 us
    pallas_call x1, Pallas kernels: 59 us -> 58.3 us  [body(): pl.pallas_call(functools.partial(kernel, n_kv, n_tp, feats * n_kv), out_s...]
where the time goes in v2:
time: 61.8 us; the launch traced here: 61.6 us
  Pallas kernels  58.3 us (94%)
  local copies, waits for them, and re-layouts  2.64 us (4%)
  between operations  0.64 us (1%)
    pallas_call x1, Pallas kernels, body(): pl.pallas_call(functools.partial(kernel, n_kv, n_tp, feats * n_kv), out_s...  58.3 us
    unnamed x2, local copies, waits for them, and re-layouts  2.64 us

profile of v2, /device:TPU:1, one launch (start us, length us, event | category | flops | bytes accessed | tf_op | source)
XLA Modules:
  0.0 61.6 jit_solution(4380507642883123412)
XLA Ops:
  0.6 58.3 %shard_map.158 = (bf16[128,256]{1,0:T(8,128)(2,1)S(1)}, f32[16,2,128,256]{3,2,1,0:T(8,128)S(1)}) custom-call(bf16[128,256]{1,0:T(8,128)(2,1)} %tokens_ref.1, bf16[256]{0:T(256)(128)(2,1)} %norm_gain_ref.1, bf16[256,256]{1,0:T(8,128)(2,1)} %wq_hbm.1, bf16[256,256]{1,0:T(8,128)(2,1)} %wk_hbm.1, bf16[256,512]{1,0:T(8,128)(2,1)} %wv_hbm.1, ...), custom_call_target="tpu_custom_call" | custom-call | tf_op jit(solution)/shard_map/pallas_call | solution.py:475
  59.0 0.6 %copy.19 = bf16[128,256]{1,0:T(8,128)(2,1)} copy(bf16[128,256]{1,0:T(8,128)(2,1)S(1)} %get-tuple-element.2) | data formatting | bytes 131072
  59.6 2.0 %copy.20 = f32[16,2,128,256]{3,2,1,0:T(8,128)} copy(f32[16,2,128,256]{3,2,1,0:T(8,128)S(1)} %get-tuple-element.3) | data formatting | bytes 8388608
